TPU v7x, 32 devices: a whole 2x2x4 slice. The times are simulated.
32 devices in a mesh: grp: 2 (over y), fs: 4 (over z), tp: 4 (over x, core).
Axes of the slice: x: 2, y: 2, z: 4, core: 2. Of those that a mesh axis runs over, the one named last changes fastest.
Arguments:
- tokens: bfloat16 [8, 1024, 2048], P(('grp', 'fs'), None, 'tp'), parts along dimension 0, may hold values from -6 to 6
- mix_gain: float32 [2048], replicated, may hold values from 0.1 to 1.9
- in_matrix: float32 [2048, 1024], P('fs', 'tp'), may hold values from -0.125 to 0.125
- in_scale: float32 [1, 1024], P(None, 'tp'), may hold values from 0.5 to 2
- pool_mix: bfloat16 [8, 128, 128], P('tp'), may hold values from -0.5 to 0.5
- pool_scale: float32 [1, 1024], P(None, 'tp'), may hold values from 0.1 to 1.9
- out_matrix: float32 [1024, 2048], P('tp', 'fs'), may hold values from -0.25 to 0.25
- out_scale: float32 [1, 2048], P(None, 'fs'), may hold values from 0.5 to 2
- ffn_gain: float32 [2048], replicated, may hold values from 0.1 to 1.9
- gate_matrix: float32 [2048, 5632], P('fs', 'tp'), may hold values from -0.125 to 0.125
- gate_scale: float32 [1, 5632], P(None, 'tp'), may hold values from 0.5 to 2
- up_matrix: float32 [2048, 5632], P('fs', 'tp'), may hold values from -0.125 to 0.125
- up_scale: float32 [1, 5632], P(None, 'tp'), may hold values from 0.5 to 2
- gate_taps: float32 [3, 5632], P(None, 'tp'), may hold values from -4 to 4
- up_taps: float32 [3, 5632], P(None, 'tp'), may hold values from -4 to 4
- down_matrix: float32 [5632, 2048], P('tp', 'fs'), may hold values from -0.109375 to 0.109375
- down_scale: float32 [1, 2048], P(None, 'fs'), may hold values from 0.5 to 2
Outputs:
- layer_out: bfloat16 [8, 1024, 2048], P(('grp', 'fs'), None, 'tp'), parts along dimension 0
There are 2 independent parts, one for each index of `grp`. A program takes and returns all parts, laid end to end along the dimension named above; an argument that names none is the same for every part. Nothing has to cross between parts.
All inputs are finite; a program needn't handle non-finite values.
Results may differ from a plain program's by a relative error of at most 0.025.
Values may be sent and summed in bfloat16 or wider, within the bound.
No kernel may reach another device: no remote copies, remote signals or barrier semaphores. Data moves between devices by JAX's collectives and lax.ppermute only.
A program may use at most 128 MiB of HBM per device.

v0:
```python
import jax
import jax.numpy as jnp
from jax import lax
from jax.sharding import PartitionSpec as P

BLOCKS = 8
eps = 1e-06
widest_span = 16


def norm_rows(tok_rows, norm_gain):
    values = tok_rows.astype(jnp.float32)
    scaled = values * lax.rsqrt(jnp.mean(values * values, axis=-1, keepdims=True) + eps)
    return (scaled * norm_gain).astype(jnp.bfloat16)


def span_widths(block_ids):
    return jnp.left_shift(jnp.ones_like(block_ids), 1 + 4 * block_ids // BLOCKS)


def trailing_gap(projected, windows):
    values = projected.astype(jnp.float32)
    length = values.shape[0]
    running = values
    for offset in range(1, widest_span):
        shifted = jnp.pad(values[: length - offset], ((offset, 0), (0, 0)))
        running = running + jnp.where(windows[None, :] > offset, shifted, jnp.zeros_like(shifted))
    positions = jnp.arange(length, dtype=jnp.int32)[:, None]
    counts = jnp.minimum(positions + 1, windows[None, :]).astype(jnp.float32)
    return (running / counts - values).astype(jnp.bfloat16)


def causal_taps(linear, tap_table):
    values = linear.astype(jnp.float32)
    length = values.shape[0]
    back_one = jnp.pad(values[: length - 1], ((1, 0), (0, 0)))
    back_two = jnp.pad(values[: length - 2], ((2, 0), (0, 0)))
    return tap_table[2] * values + tap_table[1] * back_one + tap_table[0] * back_two


def fold_rows(operand, portion):
    return jnp.dot(operand, portion, preferred_element_type=jnp.float32)


def shards(
    tokens,
    mix_gain,
    in_matrix,
    in_scale,
    pool_mix,
    pool_scale,
    out_matrix,
    out_scale,
    ffn_gain,
    gate_matrix,
    gate_scale,
    up_matrix,
    up_scale,
    gate_taps,
    up_taps,
    down_matrix,
    down_scale,
):
    length = tokens.shape[1]
    own_width = tokens.shape[2]
    local_rows = tokens.reshape(length, own_width)
    gathered = lax.all_gather(local_rows, "tp", axis=1, tiled=True)
    normed = norm_rows(gathered, mix_gain)
    width_in = in_matrix.shape[1]
    in_total = fold_rows(
        normed, lax.all_gather(in_matrix.astype(jnp.bfloat16), "fs", axis=0, tiled=True)
    )
    projected = (in_total * in_scale).astype(jnp.bfloat16)
    local_blocks = pool_mix.shape[0]
    block_width = pool_mix.shape[1]
    block_ids = lax.axis_index("tp") * local_blocks + jnp.arange(local_blocks, dtype=jnp.int32)
    windows = jnp.repeat(span_widths(block_ids), block_width)
    spread = trailing_gap(projected, windows)
    block_mixed = jnp.einsum(
        "lbc,bce->lbe",
        spread.reshape(length, local_blocks, block_width),
        pool_mix,
        preferred_element_type=jnp.float32,
    ).reshape(length, width_in)
    pooled = (block_mixed * pool_scale).astype(jnp.bfloat16)
    out_cols = lax.all_gather(out_scale, "fs", axis=1, tiled=True)
    tp_index = lax.axis_index("tp")
    groups = lax.axis_size("tp")
    pooled_all = lax.all_gather(pooled, "tp", axis=1, tiled=True)
    row_block = lax.all_gather(out_matrix.astype(jnp.bfloat16), "fs", axis=1, tiled=True)
    own_matrix = lax.all_to_all(row_block, "tp", split_axis=1, concat_axis=0, tiled=True)
    own_scales = lax.dynamic_slice_in_dim(out_cols, tp_index * own_width, own_width, 1)
    grouped_rows = pooled_all.reshape(length, groups, width_in)
    grouped_matrix = own_matrix.reshape(groups, width_in, own_width)
    pieces = (
        jnp.einsum("lgc,gcd->gld", grouped_rows, grouped_matrix, preferred_element_type=jnp.float32)
        * own_scales[None]
    )
    rounded = lax.optimization_barrier(pieces.astype(jnp.bfloat16))
    mixing = jnp.sum(rounded.astype(jnp.float32), axis=0)
    residual = (local_rows.astype(jnp.float32) + mixing).astype(jnp.bfloat16)
    gathered_ffn = lax.all_gather(residual, "tp", axis=1, tiled=True)
    normed_ffn = norm_rows(gathered_ffn, ffn_gain)
    gate_cast = gate_matrix.astype(jnp.bfloat16)
    up_cast = up_matrix.astype(jnp.bfloat16)
    gate_full, up_full = (
        lax.all_gather(gate_cast, "fs", axis=0, tiled=True),
        lax.all_gather(up_cast, "fs", axis=0, tiled=True),
    )
    gate_total = jnp.dot(normed_ffn, gate_full, preferred_element_type=jnp.float32)
    up_total = jnp.dot(normed_ffn, up_full, preferred_element_type=jnp.float32)
    gate_lin = (gate_total * gate_scale).astype(jnp.bfloat16)
    up_lin = (up_total * up_scale).astype(jnp.bfloat16)
    hidden = (jax.nn.silu(causal_taps(gate_lin, gate_taps)) * causal_taps(up_lin, up_taps)).astype(
        jnp.bfloat16
    )
    down_cols = lax.all_gather(down_scale, "fs", axis=1, tiled=True)
    partial_ffn = (
        jnp.dot(
            hidden,
            lax.all_gather(down_matrix.astype(jnp.bfloat16), "fs", axis=1, tiled=True),
            preferred_element_type=jnp.float32,
        )
        * down_cols
    )
    feed_out = lax.psum_scatter(
        partial_ffn.astype(jnp.bfloat16), "tp", scatter_dimension=1, tiled=True
    ).astype(jnp.float32)
    result = (residual.astype(jnp.float32) + feed_out).astype(jnp.bfloat16)
    return result.reshape(1, length, result.shape[1])


def solution(mesh):
    return jax.shard_map(
        shards,
        mesh=mesh,
        in_specs=(
            P(("grp", "fs"), None, "tp"),
            P(),
            P("fs", "tp"),
            P(None, "tp"),
            P("tp", None, None),
            P(None, "tp"),
            P("tp", "fs"),
            P(None, "fs"),
            P(),
            P("fs", "tp"),
            P(None, "tp"),
            P("fs", "tp"),
            P(None, "tp"),
            P(None, "tp"),
            P(None, "tp"),
            P("tp", "fs"),
            P(None, "fs"),
        ),
        out_specs=P(("grp", "fs"), None, "tp"),
        check_vma=False,
    )
```

profile of v0, /device:TPU:0, one launch (start us, length us, event | category | flops | bytes accessed | tf_op | source)
XLA Modules:
  0.0 573.4 jit_solution(17679194408588764987)
XLA Ops:
  6.5 0.7 all-gather.24.cloned.1.call-update
  7.3 0.0 all-gather.10.cloned.1.call-start
  7.3 1.8 convert_element_type.120
  9.1 0.0 all-gather.10.cloned.1.call-update
  9.1 0.0 all-gather.14.cloned.1.call-start
  9.2 1.9 copy.22
  11.0 0.0 all-gather.14.cloned.1.call-update
  11.1 0.0 all-gather.12.cloned.1.call-start
  11.1 0.1 bitcast_compare_fusion.14
  11.2 0.1 broadcast_bitcast_fusion
  11.3 34.8 %all-gather.24.cloned.1.call-done = bf16[1,1024,2048]{2,1,0:T(8,128)(2,1)} async-done(((bf16[1,1024,512]{2,1,0:T(8,128)(2,1)}), bf16[1,1024,2048]{2,1,0:T(8,128)(2,1)}) %all-gather.24.cloned.1.call-update) | async-done | bytes 4194320 | tf_op jit(solution)/shard_map/all_gather | solution.py:67
  46.1 3.1 fusion.3
  49.2 26.5 %all-gather.10.cloned.1.call-done = bf16[2048,256]{1,0:T(8,128)(2,1)} async-done(((bf16[512,256]{1,0:T(8,128)(2,1)}), bf16[2048,256]{1,0:T(8,128)(2,1)}) %all-gather.10.cloned.1.call-update) | async-done | bytes 1048592 | tf_op jit(solution)/shard_map/all_gather | solution.py:71
  75.7 3.8 fusion.20
  79.5 0.1 slice.107
  79.6 0.1 slice.108
  79.7 0.1 slice.109
  79.7 0.1 slice.110
  79.8 0.1 slice.111
  79.9 0.1 slice.112
  80.0 0.1 slice.113
  80.0 0.1 slice.114
  80.1 0.0 copy-start.12
  80.1 3.2 fusion.28
  83.4 0.0 copy-start.10
  83.4 0.9 fusion.26
  84.3 0.0 all-gather.12.cloned.1.call-update
  84.3 20.3 %all-gather.14.cloned.1.call-done = bf16[256,2048]{0,1:T(8,128)(2,1)} async-done(((bf16[256,512]{0,1:T(8,128)(2,1)}), bf16[256,2048]{0,1:T(8,128)(2,1)}) %all-gather.14.cloned.1.call-update) | async-done | bytes 1048592 | tf_op jit(solution)/shard_map/all_gather | solution.py:90
  104.7 2.3 copy.23
  106.9 3.5 all-to-all-start
  110.5 0.0 all-gather.16.cloned.1.call-start
  110.5 11.9 %all_gather.34 = f32[1,2048]{1,0:T(1,128)S(1)} all-gather(f32[1,512]{1,0:T(1,128)S(1)} %copy-done.10), channel_id=1, replica_groups=mesh['grp'=2,'fs'=4,'tp'=4] {'fs'}, dimensions={1}, use_global_device_ids=true | all-gather | bytes 10240 | tf_op jit(solution)/shard_map/all_gather | solution.py:86
  122.5 12.5 %all-to-all-done = bf16[256,4,512]{2,0,1:T(8,128)(2,1)S(1)} async-done(((bf16[256,4,512]{2,0,1:T(8,128)(2,1)}), bf16[256,4,512]{2,0,1:T(8,128)(2,1)S(1)}, u32[]{:S(2)}, u32[]{:S(2)}) %all-to-all-start) | async-done | bytes 1048608 | tf_op jit(solution)/shard_map/all_to_all | solution.py:91
  135.0 2.7 all-gather.12.cloned.1.call-done
  137.6 3.0 multiply_convert_fusion.1
  140.6 0.0 copy-start.4
  140.6 0.7 convert_reduce_fusion
  141.3 1.3 fusion.13
  142.6 0.0 all-gather.16.cloned.1.call-update
  142.7 0.0 all-gather.18.cloned.1.call-start
  142.7 1.3 convert_element_type.133
  144.0 0.0 all-gather.18.cloned.1.call-update
  144.1 0.0 copy-start.9
  144.1 0.0 copy-start.11
  144.1 0.0 all-gather.20.cloned.1.call-start
  144.2 3.3 convert_element_type.136
  147.5 0.0 all-gather.20.cloned.1.call-update
  147.5 0.0 all-gather.22.cloned.1.call-start
  147.5 1.3 convert_element_type.140
  148.8 0.0 all-gather.22.cloned.1.call-update
  148.8 0.0 reduce-scatter.2.cloned.1.call-start
  149.0 12.1 %all_gather.39 = f32[1,2048]{1,0:T(1,128)S(1)} all-gather(f32[1,512]{1,0:T(1,128)S(1)} %copy-done.11), channel_id=1, replica_groups=mesh['grp'=2,'fs'=4,'tp'=4] {'fs'}, dimensions={1}, use_global_device_ids=true | all-gather | bytes 10240 | tf_op jit(solution)/shard_map/all_gather | solution.py:117
  161.1 0.1 slice_reduce_fusion.2
  161.2 14.5 %all-gather.16.cloned.1.call-done = bf16[1024,2048]{1,0:T(8,128)(2,1)} async-done(((bf16[1024,512]{1,0:T(8,128)(2,1)}), bf16[1024,2048]{1,0:T(8,128)(2,1)}) %all-gather.16.cloned.1.call-update) | async-done | bytes 4194320 | tf_op jit(solution)/shard_map/all_gather | solution.py:102
  175.7 3.1 fusion
  178.8 105.1 %all-gather.18.cloned.1.call-done = bf16[2048,1408]{1,0:T(8,128)(2,1)} async-done(((bf16[512,1408]{1,0:T(8,128)(2,1)}), bf16[2048,1408]{1,0:T(8,128)(2,1)}) %all-gather.18.cloned.1.call-update) | async-done | bytes 5767184 | tf_op jit(solution)/shard_map/all_gather | solution.py:107
  283.9 11.9 %fusion.11 = f32[1024,1408]{1,0:T(8,128)} fusion(bf16[2048,1408]{1,0:T(8,128)(2,1)} %all-gather.18.cloned.1.call-done, f32[1408]{0:T(1024)S(1)} %reduce.1, bf16[1024,2048]{1,0:T(8,128)(2,1)} %all-gather.16.cloned.1.call-done, f32[2048]{0:T(1024)S(1)} %copy-done.14, f32[1024]{0:T(1024)S(1)} %add_rsqrt_fusion), kind=kOutput, calls=%fused_computation.20 | convolution fusion | flops 5918294016 | bytes 15746560 | tf_op jit(solution)/shard_map/dot_general | solution.py:110
  295.8 94.7 %all-gather.20.cloned.1.call-done = bf16[2048,1408]{1,0:T(8,128)(2,1)} async-done(((bf16[512,1408]{1,0:T(8,128)(2,1)}), bf16[2048,1408]{1,0:T(8,128)(2,1)}) %all-gather.20.cloned.1.call-update) | async-done | bytes 5767184 | tf_op jit(solution)/shard_map/all_gather | solution.py:108
  390.4 12.0 %fusion.12 = f32[1024,1408]{1,0:T(8,128)} fusion(bf16[2048,1408]{1,0:T(8,128)(2,1)} %all-gather.20.cloned.1.call-done, f32[1408]{0:T(1024)S(1)} %reduce.5, bf16[1024,2048]{1,0:T(8,128)(2,1)} %all-gather.16.cloned.1.call-done, f32[2048]{0:T(1024)S(1)} %copy-done.14, f32[1024]{0:T(1024)S(1)} %add_rsqrt_fusion), kind=kOutput, calls=%fused_computation.21 | convolution fusion | flops 5918294016 | bytes 15746560 | tf_op jit(solution)/shard_map/dot_general | solution.py:111
  402.4 94.6 %all-gather.22.cloned.1.call-done = bf16[1408,2048]{1,0:T(8,128)(2,1)} async-done(((bf16[1408,512]{1,0:T(8,128)(2,1)}), bf16[1408,2048]{1,0:T(8,128)(2,1)}) %all-gather.22.cloned.1.call-update) | async-done | bytes 5767184 | tf_op jit(solution)/shard_map/all_gather | solution.py:121
  497.0 24.6 %multiply_convert_fusion = bf16[1024,2048]{1,0:T(8,128)(2,1)} fusion(bf16[1408,2048]{1,0:T(8,128)(2,1)} %all-gather.22.cloned.1.call-done, f32[2048]{0:T(1024)S(1)} %bitcast.83, f32[1022,1408]{1,0:T(8,128)} %bitcast.89, f32[1023,1408]{1,0:T(8,128)} %bitcast.90, f32[1024,1408]{1,0:T(8,128)} %fusion.12, f32[1022,1408]{1,0:T(8,128)} %bitcast.87, ...), kind=kOutput, calls=%fused_computation.10 | convolution fusion | flops 5932843008 | bytes 44572672 | tf_op jit(solution)/shard_map/dot_general | solution.py:119
  521.6 0.0 reduce-scatter.2.cloned.1.call-update
  521.6 42.8 %reduce-scatter.2.cloned.1.call-done = bf16[1024,512]{1,0:T(8,128)(2,1)} async-done(((bf16[1024,2048]{1,0:T(8,128)(2,1)}), bf16[1024,512]{1,0:T(8,128)(2,1)}) %reduce-scatter.2.cloned.1.call-update) | async-done | bytes 1048592 | tf_op jit(solution)/shard_map/reduce_scatter | solution.py:126
  564.4 2.5 fusion.25
  (35 shorter events, 0.1 us)
Async XLA Ops:
  6.5 73.6 %copy-start = (bf16[2,128,128]{2,1,0:T(8,128)(2,1)S(1)}, bf16[2,128,128]{2,1,0:T(8,128)(2,1)}, u32[]{:S(2)}) copy-start(bf16[2,128,128]{2,1,0:T(8,128)(2,1)} %param.21) | copy-start | bytes 196612
  6.5 69.2 %copy-start.15 = (f32[1,256]{1,0:T(1,128)S(1)}, f32[1,256]{1,0:T(1,128)}, u32[]{:S(2)}) copy-start(f32[1,256]{1,0:T(1,128)} %param.20) | copy-start | bytes 3076
  6.5 69.2 %copy-start.13 = (f32[2048]{0:T(1024)S(1)}, f32[2048]{0:T(1024)}, u32[]{:S(2)}) copy-start(f32[2048]{0:T(1024)} %param.18) | copy-start | bytes 24580
  6.5 39.6 %all-gather.24.cloned.1.call-start = ((), (), s32[]{:S(2)}) async-start(), calls=%async_computation.10 | async-start | bytes 5242880 | tf_op jit(solution)/shard_map/all_gather | solution.py:67
  7.3 68.4 %all-gather.10.cloned.1.call-start = ((), (), s32[]{:S(2)}) async-start(), calls=%async_computation.2 | async-start | bytes 1310720 | tf_op jit(solution)/shard_map/all_gather | solution.py:71
  9.1 95.6 %all-gather.14.cloned.1.call-start = ((), (), s32[]{:S(2)}) async-start(), calls=%async_computation.4 | async-start | bytes 1310720 | tf_op jit(solution)/shard_map/all_gather | solution.py:90
  11.1 126.6 %all-gather.12.cloned.1.call-start = ((), (), s32[]{:S(2)}) async-start(), calls=%async_computation.3 | async-start | bytes 2621440 | tf_op jit(solution)/shard_map/all_gather | solution.py:89
  80.1 3.3 copy-start.12
  83.4 27.1 %copy-start.10 = (f32[1,512]{1,0:T(1,128)S(1)}, f32[1,512]{1,0:T(1,128)}, u32[]{:S(2)}) copy-start(f32[1,512]{1,0:T(1,128)} %param.24) | copy-start | bytes 6148
  106.9 28.0 %all-to-all-start = ((bf16[256,4,512]{2,0,1:T(8,128)(2,1)}), bf16[256,4,512]{2,0,1:T(8,128)(2,1)S(1)}, u32[]{:S(2)}, u32[]{:S(2)}) async-start(bf16[256,4,512]{2,0,1:T(8,128)(2,1)} %copy.23), calls=%async_computation | async-start | bytes 2097152 | tf_op jit(solution)/shard_map/all_to_all | solution.py:91
  110.5 65.3 %all-gather.16.cloned.1.call-start = ((), (), s32[]{:S(2)}) async-start(), calls=%async_computation.5 | async-start | bytes 5242880 | tf_op jit(solution)/shard_map/all_gather | solution.py:102
  137.6 3.7 copy-start.3
  140.6 2.1 copy-start.4
  142.7 141.2 %all-gather.18.cloned.1.call-start = ((), (), s32[]{:S(2)}) async-start(), calls=%async_computation.6 | async-start | bytes 7208960 | tf_op jit(solution)/shard_map/all_gather | solution.py:107
  144.0 3.5 copy-start.5
  144.1 4.8 copy-start.8
  144.1 4.9 copy-start.9
  144.1 4.9 copy-start.11
  144.1 17.0 %copy-start.6 = (f32[3,1408]{1,0:T(4,128)S(1)}, f32[3,1408]{1,0:T(4,128)}, u32[]{:S(2)}) copy-start(f32[3,1408]{1,0:T(4,128)} %param.31) | copy-start | bytes 50692
  144.1 17.0 %copy-start.7 = (f32[3,1408]{1,0:T(4,128)S(1)}, f32[3,1408]{1,0:T(4,128)}, u32[]{:S(2)}) copy-start(f32[3,1408]{1,0:T(4,128)} %param.30) | copy-start | bytes 50692
  144.1 246.3 %all-gather.20.cloned.1.call-start = ((), (), s32[]{:S(2)}) async-start(), calls=%async_computation.7 | async-start | bytes 7208960 | tf_op jit(solution)/shard_map/all_gather | solution.py:108
  147.5 136.4 %copy-start.14 = (f32[2048]{0:T(1024)S(1)}, f32[2048]{0:T(1024)}, u32[]{:S(2)}) copy-start(f32[2048]{0:T(1024)} %param.25) | copy-start | bytes 24580
  147.5 349.5 %all-gather.22.cloned.1.call-start = ((), (), s32[]{:S(2)}) async-start(), calls=%async_computation.8 | async-start | bytes 7208960 | tf_op jit(solution)/shard_map/all_gather | solution.py:121
  148.8 415.6 %reduce-scatter.2.cloned.1.call-start = ((), (), s32[]{:S(2)}) async-start(), calls=%async_computation.9 | async-start | bytes 5242880 | tf_op jit(solution)/shard_map/reduce_scatter | solution.py:126
  497.0 67.4 %copy-start.2 = (bf16[1024,512]{1,0:T(8,128)(2,1)S(1)}, bf16[1024,512]{1,0:T(8,128)(2,1)}, u32[]{:S(2)}) copy-start(bf16[1024,512]{1,0:T(8,128)(2,1)} %fusion.13) | copy-start | bytes 3145732
  497.0 69.9 %copy-start.1 = (bf16[2,128,128]{2,1,0:T(8,128)(2,1)S(1)}, bf16[2,128,128]{2,1,0:T(8,128)(2,1)}, u32[]{:S(2)}) copy-start(bf16[2,128,128]{2,1,0:T(8,128)(2,1)} %param.21) | copy-start | bytes 196612
Sparse Core Ops, SparseCore 0:
  8.9 37.1 all-gather.23
  47.7 27.9 all-gather.9
  77.3 27.3 all-gather.13
  106.1 31.4 all-gather.11
  142.8 32.9 all-gather.15
  177.2 106.6 all-gather.17
  285.5 104.9 all-gather.19
  392.0 104.9 all-gather.21
  521.8 42.6 reduce-scatter.1
where the time goes:
time: 574 us; the launch traced here: 573 us
  waiting for transfers between devices  449 us (78%)
  matrix products  58.5 us (10%)
  blocking collectives  24.1 us (4%)
  other arithmetic  19.3 us (3%)
  between operations  13.5 us (2%)
    all_gather x1, waiting for transfers between devices, shards(): lax.all_gather(gate_cast, 'fs', axis=0, tiled=True)  105 us
    all_gather x1, waiting for transfers between devices, shards(): lax.all_gather(up_cast, 'fs', axis=0, tiled=True)  94.7 us
    all_gather x1, waiting for transfers between devices, shards(): lax.all_gather(down_matrix.astype(jnp.bfloat16), 'fs', axis=1, tiled=True)  94.6 us
    reduce_scatter x1, waiting for transfers between devices, shards(): lax.psum_scatter(partial_ffn.astype(jnp.bfloat16), 'tp', scatter_dimensio...  42.8 us
    all_gather x1, waiting for transfers between devices, shards(): gathered = lax.all_gather(local_rows, 'tp', axis=1, tiled=True)  34.8 us
    all_gather x1, waiting for transfers between devices, shards(): lax.all_gather(in_matrix.astype(jnp.bfloat16), 'fs', axis=0, tiled=True)  26.5 us
    dot_general x1, matrix products, shards(): jnp.dot(hidden, lax.all_gather(down_matrix.astype(jnp.bfloat16), 'fs', ax...  24.6 us
    all_gather x1, waiting for transfers between devices, shards(): lax.all_gather(out_matrix.astype(jnp.bfloat16), 'fs', axis=1, tiled=True)  20.3 us
  transfers between devices with their start and end apart: 10, of which 10 were waited for; matrix products, arithmetic and copies ran while one was open for 9% of the time, Pallas kernels for 0%

commit v1 on v0

--- a/solution.py
+++ b/solution.py
@@ -64,7 +64,12 @@
     length = tokens.shape[1]
     own_width = tokens.shape[2]
     local_rows = tokens.reshape(length, own_width)
-    gathered = lax.all_gather(local_rows, "tp", axis=1, tiled=True)
+    ring = [local_rows]
+    for hop in range(3):
+        ring.append(lax.ppermute(ring[-1], "tp", [(dev, (dev + 1) % 4) for dev in range(4)]))
+    gathered = jnp.roll(
+        jnp.concatenate(ring[::-1], axis=1), (lax.axis_index("tp") + 1) * ring[0].shape[1], axis=1
+    )
     normed = norm_rows(gathered, mix_gain)
     width_in = in_matrix.shape[1]
     in_total = fold_rows(

time: 574 us -> 539 us (0.939)
  waiting for transfers between devices: 449 us -> 407 us
  local copies, waits for them, and re-layouts: 4.94 us -> 11.8 us
    ppermute x0 -> x3, waiting for transfers between devices: none -> 39.2 us  [shards(): lax.ppermute(ring[-1], 'tp', [(dev, (dev + 1) % 4) for dev in range(4)])]
    all_gather x1 -> x0, waiting for transfers between devices: 34.8 us -> none  [shards(): gathered = lax.all_gather(local_rows, 'tp', axis=1, tiled=True)]
    all_gather x1, waiting for transfers between devices: 26.5 us -> 0.02 us  [shards(): lax.all_gather(in_matrix.astype(jnp.bfloat16), 'fs', axis=0, tiled=True)]
    all_gather x1, waiting for transfers between devices: 20.3 us -> 1.77 us  [shards(): lax.all_gather(out_matrix.astype(jnp.bfloat16), 'fs', axis=1, tiled=True)]
    unnamed x33 -> x40, local copies, waits for them, and re-layouts: 1.96 us -> 8.7 us
  transfers between devices with their start and end apart: 10 -> 12, of which waited for: 10 -> 11; matrix products, arithmetic and copies ran while one was open for 9% -> 10% of each run, Pallas kernels for 0% -> 0%
where the time goes in v1:
time: 539 us; the launch traced here: 538 us
  waiting for transfers between devices  407 us (76%)
  matrix products  58.5 us (11%)
  blocking collectives  24.1 us (4%)
  other arithmetic  19.2 us (4%)
  between operations  13.9 us (3%)
  local copies, waits for them, and re-layouts  11.8 us (2%)
    all_gather x1, waiting for transfers between devices, shards(): lax.all_gather(gate_cast, 'fs', axis=0, tiled=True)  105 us
    all_gather x1, waiting for transfers between devices, shards(): lax.all_gather(down_matrix.astype(jnp.bfloat16), 'fs', axis=1, tiled=True)  94.6 us
    all_gather x1, waiting for transfers between devices, shards(): lax.all_gather(up_cast, 'fs', axis=0, tiled=True)  94.5 us
    reduce_scatter x1, waiting for transfers between devices, shards(): lax.psum_scatter(partial_ffn.astype(jnp.bfloat16), 'tp', scatter_dimensio...  42.8 us
    ppermute x3, waiting for transfers between devices, shards(): lax.ppermute(ring[-1], 'tp', [(dev, (dev + 1) % 4) for dev in range(4)])  39.2 us
    dot_general x1, matrix products, shards(): jnp.dot(hidden, lax.all_gather(down_matrix.astype(jnp.bfloat16), 'fs', ax...  24.6 us
    all_gather x1, waiting for transfers between devices, shards(): gathered_ffn = lax.all_gather(residual, 'tp', axis=1, tiled=True)  13.4 us
    all_to_all x1, waiting for transfers between devices, shards(): lax.all_to_all(row_block, 'tp', split_axis=1, concat_axis=0, tiled=True)  12.3 us
  transfers between devices with their start and end apart: 12, of which 11 were waited for; matrix products, arithmetic and copies ran while one was open for 10% of the time, Pallas kernels for 0%

profile of v1, /device:TPU:0, one launch (start us, length us, event | category | flops | bytes accessed | tf_op | source)
XLA Modules:
  0.0 538.3 jit_solution(614038206354753600)
XLA Ops:
  6.5 0.5 collective-permute-start
  7.0 1.8 convert_element_type.120
  8.8 0.0 all-gather.8.cloned.1.call-update
  8.8 0.0 all-gather.12.cloned.1.call-start
  8.9 12.8 %collective-permute-done = bf16[1024,512]{1,0:T(8,128)(2,1)S(1)} collective-permute-done((bf16[1024,512]{1,0:T(8,128)(2,1)}, bf16[1024,512]{1,0:T(8,128)(2,1)S(1)}, u32[]{:S(2)}, u32[]{:S(2)}) %collective-permute-start) | collective-permute-done | bytes 1048608 | tf_op jit(solution)/shard_map/ppermute | solution.py:69
  21.7 14.2 %collective-permute-done.1 = bf16[1024,512]{1,0:T(8,128)(2,1)S(1)} collective-permute-done((bf16[1024,512]{1,0:T(8,128)(2,1)S(1)}, bf16[1024,512]{1,0:T(8,128)(2,1)S(1)}, u32[]{:S(2)}, u32[]{:S(2)}) %collective-permute-start.1) | collective-permute-done | bytes 1048608 | tf_op jit(solution)/shard_map/ppermute | solution.py:69
  35.9 1.9 copy.22
  37.8 0.0 all-gather.12.cloned.1.call-update
  37.8 0.0 all-gather.10.cloned.1.call-start
  37.9 0.1 broadcast_bitcast_fusion
  38.0 0.1 bitcast_compare_fusion.14
  38.1 12.2 %collective-permute-done.2 = bf16[1024,512]{1,0:T(8,128)(2,1)} collective-permute-done((bf16[1024,512]{1,0:T(8,128)(2,1)S(1)}, bf16[1024,512]{1,0:T(8,128)(2,1)}, u32[]{:S(2)}, u32[]{:S(2)}) %collective-permute-start.2) | collective-permute-done | bytes 1048608 | tf_op jit(solution)/shard_map/ppermute | solution.py:69
  50.2 1.4 constant_dynamic-update-slice_fusion.7
  51.6 0.2 constant_dynamic-update-slice_fusion.6
  51.8 0.2 constant_dynamic-update-slice_fusion.5
  51.9 0.1 constant_dynamic-update-slice_fusion.4
  52.1 1.4 constant_dynamic-update-slice_fusion.3
  53.5 0.1 constant_dynamic-update-slice_fusion.2
  53.7 0.2 constant_dynamic-update-slice_fusion.1
  53.8 0.2 constant_dynamic-update-slice_fusion
  54.0 3.2 copy-done.4
  57.2 0.9 fusion
  58.1 0.0 all-gather.8.cloned.1.call-done
  58.2 3.8 fusion.19
  62.0 0.1 slice.107
  62.1 0.1 slice.108
  62.2 0.1 slice.109
  62.2 0.1 slice.110
  62.3 0.1 slice.111
  62.4 0.1 slice.112
  62.5 0.1 slice.113
  62.5 0.1 slice.114
  62.6 3.2 fusion.27
  65.9 0.9 fusion.25
  66.8 0.0 all-gather.10.cloned.1.call-update
  66.8 1.8 all-gather.12.cloned.1.call-done
  68.6 2.3 copy.23
  70.9 3.5 all-to-all-start
  74.4 0.0 all-gather.14.cloned.1.call-start
  74.5 11.9 %all_gather.30 = f32[1,2048]{1,0:T(1,128)S(1)} all-gather(f32[1,512]{1,0:T(1,128)S(1)} %copy-done.10), channel_id=1, replica_groups=mesh['grp'=2,'fs'=4,'tp'=4] {'fs'}, dimensions={1}, use_global_device_ids=true | all-gather | bytes 10240 | tf_op jit(solution)/shard_map/all_gather | solution.py:91
  86.4 12.3 %all-to-all-done = bf16[256,4,512]{2,0,1:T(8,128)(2,1)S(1)} async-done(((bf16[256,4,512]{2,0,1:T(8,128)(2,1)}), bf16[256,4,512]{2,0,1:T(8,128)(2,1)S(1)}, u32[]{:S(2)}, u32[]{:S(2)}) %all-to-all-start) | async-done | bytes 1048608 | tf_op jit(solution)/shard_map/all_to_all | solution.py:96
  98.7 2.8 all-gather.10.cloned.1.call-done
  101.6 2.9 multiply_convert_fusion.1
  104.5 0.7 convert_reduce_fusion
  105.1 1.3 add_convert_fusion.1
  106.5 0.0 all-gather.16.cloned.1.call-start
  106.5 3.3 convert_element_type.133
  109.9 0.0 all-gather.18.cloned.1.call-start
  109.9 1.3 convert_element_type.136
  111.3 0.0 all-gather.20.cloned.1.call-start
  111.3 3.4 convert_element_type.140
  114.7 0.0 reduce-scatter.2.cloned.1.call-start
  114.9 12.1 %all_gather.35 = f32[1,2048]{1,0:T(1,128)S(1)} all-gather(f32[1,512]{1,0:T(1,128)S(1)} %copy-done.11), channel_id=1, replica_groups=mesh['grp'=2,'fs'=4,'tp'=4] {'fs'}, dimensions={1}, use_global_device_ids=true | all-gather | bytes 10240 | tf_op jit(solution)/shard_map/all_gather | solution.py:122
  127.0 0.1 slice_reduce_fusion.2
  127.1 13.4 %all-gather.14.cloned.1.call-done = bf16[1024,2048]{1,0:T(8,128)(2,1)} async-done(((bf16[1024,512]{1,0:T(8,128)(2,1)}), bf16[1024,2048]{1,0:T(8,128)(2,1)}) %all-gather.14.cloned.1.call-update) | async-done | bytes 4194320 | tf_op jit(solution)/shard_map/all_gather | solution.py:107
  140.4 3.1 fusion.3
  143.5 105.1 %all-gather.16.cloned.1.call-done = bf16[2048,1408]{1,0:T(8,128)(2,1)} async-done(((bf16[512,1408]{1,0:T(8,128)(2,1)}), bf16[2048,1408]{1,0:T(8,128)(2,1)}) %all-gather.16.cloned.1.call-update) | async-done | bytes 5767184 | tf_op jit(solution)/shard_map/all_gather | solution.py:112
  248.6 11.9 %fusion.10 = f32[1024,1408]{1,0:T(8,128)} fusion(bf16[2048,1408]{1,0:T(8,128)(2,1)} %all-gather.16.cloned.1.call-done, f32[1408]{0:T(1024)S(1)} %reduce.1, bf16[1024,2048]{1,0:T(8,128)(2,1)} %all-gather.14.cloned.1.call-done, f32[2048]{0:T(1024)S(1)} %copy-done.14, f32[1024]{0:T(1024)S(1)} %add_rsqrt_fusion), kind=kOutput, calls=%fused_computation.19 | convolution fusion | flops 5918294016 | bytes 15746560 | tf_op jit(solution)/shard_map/dot_general | solution.py:115
  260.5 94.5 %all-gather.18.cloned.1.call-done = bf16[2048,1408]{1,0:T(8,128)(2,1)} async-done(((bf16[512,1408]{1,0:T(8,128)(2,1)}), bf16[2048,1408]{1,0:T(8,128)(2,1)}) %all-gather.18.cloned.1.call-update) | async-done | bytes 5767184 | tf_op jit(solution)/shard_map/all_gather | solution.py:113
  355.0 12.0 %fusion.11 = f32[1024,1408]{1,0:T(8,128)} fusion(bf16[2048,1408]{1,0:T(8,128)(2,1)} %all-gather.18.cloned.1.call-done, f32[1408]{0:T(1024)S(1)} %reduce.5, bf16[1024,2048]{1,0:T(8,128)(2,1)} %all-gather.14.cloned.1.call-done, f32[2048]{0:T(1024)S(1)} %copy-done.14, f32[1024]{0:T(1024)S(1)} %add_rsqrt_fusion), kind=kOutput, calls=%fused_computation.20 | convolution fusion | flops 5918294016 | bytes 15746560 | tf_op jit(solution)/shard_map/dot_general | solution.py:116
  367.0 94.6 %all-gather.20.cloned.1.call-done = bf16[1408,2048]{1,0:T(8,128)(2,1)} async-done(((bf16[1408,512]{1,0:T(8,128)(2,1)}), bf16[1408,2048]{1,0:T(8,128)(2,1)}) %all-gather.20.cloned.1.call-update) | async-done | bytes 5767184 | tf_op jit(solution)/shard_map/all_gather | solution.py:126
  461.5 24.6 %multiply_convert_fusion = bf16[1024,2048]{1,0:T(8,128)(2,1)} fusion(bf16[1408,2048]{1,0:T(8,128)(2,1)} %all-gather.20.cloned.1.call-done, f32[2048]{0:T(1024)S(1)} %bitcast.72, f32[1022,1408]{1,0:T(8,128)} %bitcast.78, f32[1023,1408]{1,0:T(8,128)} %bitcast.79, f32[1024,1408]{1,0:T(8,128)} %fusion.11, f32[1022,1408]{1,0:T(8,128)} %bitcast.76, ...), kind=kOutput, calls=%fused_computation.10 | convolution fusion | flops 5932843008 | bytes 44572672 | tf_op jit(solution)/shard_map/dot_general | solution.py:124
  486.2 42.8 %reduce-scatter.2.cloned.1.call-done = bf16[1024,512]{1,0:T(8,128)(2,1)} async-done(((bf16[1024,2048]{1,0:T(8,128)(2,1)}), bf16[1024,512]{1,0:T(8,128)(2,1)}) %reduce-scatter.2.cloned.1.call-update) | async-done | bytes 1048592 | tf_op jit(solution)/shard_map/reduce_scatter | solution.py:131
  529.0 2.5 fusion.24
  (46 shorter events, 0.3 us)
Async XLA Ops:
  6.5 56.1 %copy-start = (bf16[2,128,128]{2,1,0:T(8,128)(2,1)S(1)}, bf16[2,128,128]{2,1,0:T(8,128)(2,1)}, u32[]{:S(2)}) copy-start(bf16[2,128,128]{2,1,0:T(8,128)(2,1)} %param.21) | copy-start | bytes 196612
  6.5 45.4 %copy-start.3 = (bf16[1,1024,512]{2,1,0:T(8,128)(2,1)S(1)}, bf16[1,1024,512]{2,1,0:T(8,128)(2,1)}, u32[]{:S(2)}) copy-start(bf16[1,1024,512]{2,1,0:T(8,128)(2,1)} %param.17) | copy-start | bytes 3145732
  6.5 51.6 %all-gather.8.cloned.1.call-start = ((), (), s32[]{:S(2)}) async-start(), calls=%async_computation.2 | async-start | bytes 1310720 | tf_op jit(solution)/shard_map/all_gather | solution.py:76
  6.5 15.1 %collective-permute-start = (bf16[1024,512]{1,0:T(8,128)(2,1)}, bf16[1024,512]{1,0:T(8,128)(2,1)S(1)}, u32[]{:S(2)}, u32[]{:S(2)}) collective-permute-start(bf16[1024,512]{1,0:T(8,128)(2,1)} %bitcast.69), channel_id=1, source_target_pairs={{0,1},{1,2},{2,3},{3,0},{4,5},{5,6},{6,7},{7,4},{8,9},{9,10},{10,1... | collective-permute-start | bytes 3145736 | tf_op jit(solution)/shard_map/ppermute | solution.py:69
  8.8 59.8 %all-gather.12.cloned.1.call-start = ((), (), s32[]{:S(2)}) async-start(), calls=%async_computation.4 | async-start | bytes 1310720 | tf_op jit(solution)/shard_map/all_gather | solution.py:95
  21.7 14.2 %collective-permute-start.1 = (bf16[1024,512]{1,0:T(8,128)(2,1)S(1)}, bf16[1024,512]{1,0:T(8,128)(2,1)S(1)}, u32[]{:S(2)}, u32[]{:S(2)}) collective-permute-start(bf16[1024,512]{1,0:T(8,128)(2,1)S(1)} %collective-permute-done), channel_id=1, source_target_pairs={{0,1},{1,2},{2,3},{3,0},{4,5},{5,6},{6,7},{7,4},{8,9},{9,10},{10,1... | collective-permute-start | bytes 3145736 | tf_op jit(solution)/shard_map/ppermute | solution.py:69
  35.9 14.3 %collective-permute-start.2 = (bf16[1024,512]{1,0:T(8,128)(2,1)S(1)}, bf16[1024,512]{1,0:T(8,128)(2,1)}, u32[]{:S(2)}, u32[]{:S(2)}) collective-permute-start(bf16[1024,512]{1,0:T(8,128)(2,1)S(1)} %collective-permute-done.1), channel_id=1, source_target_pairs={{0,1},{1,2},{2,3},{3,0},{4,5},{5,6},{6,7},{7,4},{8,9},{9,10},{10,1... | collective-permute-start | bytes 3145736 | tf_op jit(solution)/shard_map/ppermute | solution.py:69
  37.8 63.7 %all-gather.10.cloned.1.call-start = ((), (), s32[]{:S(2)}) async-start(), calls=%async_computation.3 | async-start | bytes 2621440 | tf_op jit(solution)/shard_map/all_gather | solution.py:94
  53.5 4.7 copy-start.13
  53.5 4.7 copy-start.15
  54.0 3.2 copy-start.4
  62.6 3.2 copy-start.12
  65.9 8.6 %copy-start.10 = (f32[1,512]{1,0:T(1,128)S(1)}, f32[1,512]{1,0:T(1,128)}, u32[]{:S(2)}) copy-start(f32[1,512]{1,0:T(1,128)} %param.24) | copy-start | bytes 6148
  70.9 27.9 %all-to-all-start = ((bf16[256,4,512]{2,0,1:T(8,128)(2,1)}), bf16[256,4,512]{2,0,1:T(8,128)(2,1)S(1)}, u32[]{:S(2)}, u32[]{:S(2)}) async-start(bf16[256,4,512]{2,0,1:T(8,128)(2,1)} %copy.23), calls=%async_computation | async-start | bytes 2097152 | tf_op jit(solution)/shard_map/all_to_all | solution.py:96
  74.4 66.0 %all-gather.14.cloned.1.call-start = ((), (), s32[]{:S(2)}) async-start(), calls=%async_computation.5 | async-start | bytes 5242880 | tf_op jit(solution)/shard_map/all_gather | solution.py:107
  106.4 3.5 copy-start.5
  106.5 142.1 %all-gather.16.cloned.1.call-start = ((), (), s32[]{:S(2)}) async-start(), calls=%async_computation.6 | async-start | bytes 7208960 | tf_op jit(solution)/shard_map/all_gather | solution.py:112
  109.8 5.0 copy-start.8
  109.8 5.0 copy-start.9
  109.8 5.0 copy-start.11
  109.9 17.1 %copy-start.6 = (f32[3,1408]{1,0:T(4,128)S(1)}, f32[3,1408]{1,0:T(4,128)}, u32[]{:S(2)}) copy-start(f32[3,1408]{1,0:T(4,128)} %param.31) | copy-start | bytes 50692
  109.9 17.1 %copy-start.7 = (f32[3,1408]{1,0:T(4,128)S(1)}, f32[3,1408]{1,0:T(4,128)}, u32[]{:S(2)}) copy-start(f32[3,1408]{1,0:T(4,128)} %param.30) | copy-start | bytes 50692
  109.9 245.1 %all-gather.18.cloned.1.call-start = ((), (), s32[]{:S(2)}) async-start(), calls=%async_computation.7 | async-start | bytes 7208960 | tf_op jit(solution)/shard_map/all_gather | solution.py:113
  111.3 137.3 %copy-start.14 = (f32[2048]{0:T(1024)S(1)}, f32[2048]{0:T(1024)}, u32[]{:S(2)}) copy-start(f32[2048]{0:T(1024)} %param.25) | copy-start | bytes 24580
  111.3 350.2 %all-gather.20.cloned.1.call-start = ((), (), s32[]{:S(2)}) async-start(), calls=%async_computation.8 | async-start | bytes 7208960 | tf_op jit(solution)/shard_map/all_gather | solution.py:126
  114.7 414.3 %reduce-scatter.2.cloned.1.call-start = ((), (), s32[]{:S(2)}) async-start(), calls=%async_computation.9 | async-start | bytes 5242880 | tf_op jit(solution)/shard_map/reduce_scatter | solution.py:131
  461.5 67.5 %copy-start.2 = (bf16[1024,512]{1,0:T(8,128)(2,1)S(1)}, bf16[1024,512]{1,0:T(8,128)(2,1)}, u32[]{:S(2)}) copy-start(bf16[1024,512]{1,0:T(8,128)(2,1)} %add_convert_fusion.1) | copy-start | bytes 3145732
  461.5 70.0 %copy-start.1 = (bf16[2,128,128]{2,1,0:T(8,128)(2,1)S(1)}, bf16[2,128,128]{2,1,0:T(8,128)(2,1)}, u32[]{:S(2)}) copy-start(bf16[2,128,128]{2,1,0:T(8,128)(2,1)} %param.21) | copy-start | bytes 196612
Sparse Core Ops, SparseCore 0:
  8.9 30.6 all-gather.7
  41.2 27.3 all-gather.11
  70.2 31.3 all-gather.9
  106.6 33.8 all-gather.13
  141.9 106.6 all-gather.15
  250.0 104.9 all-gather.17
  356.5 104.9 all-gather.19
  486.3 42.6 reduce-scatter.1
